TPU v7x, 32 devices: a whole 2x2x4 slice. The times are simulated.
32 devices in a mesh: ep: 4 (over y, x), tp: 8 (over z, core).
Axes of the slice: x: 2, y: 2, z: 4, core: 2. Of those that a mesh axis runs over, the one named last changes fastest.
Arguments:
- hidden_in: bfloat16 [128, 4096], P('ep'), may hold values from -6 to 6
- mix_gain: float32 [4096], replicated, may hold values from 0.1 to 1.9
- w_query: bfloat16 [4096, 2048], P('ep', 'tp'), may hold values from -0.09375 to 0.09375
- w_key: bfloat16 [4096, 2048], P('ep', 'tp'), may hold values from -0.09375 to 0.09375
- w_value: bfloat16 [4096, 2048], P('ep', 'tp'), may hold values from -0.09375 to 0.09375
- w_outgate: bfloat16 [4096, 2048], P('ep', 'tp'), may hold values from -0.09375 to 0.09375
- w_gates: bfloat16 [2, 4096, 32], P(None, None, 'tp'), may hold values from -0.09375 to 0.09375
- gate_bias: float32 [2, 32], P(None, 'tp'), may hold values from -1 to 4
- state_matrix: float32 [128, 32, 64, 64], P('ep', 'tp'), may hold values from -2 to 2
- state_norm: float32 [128, 32, 64], P('ep', 'tp'), may hold values from -2 to 2
- state_max: float32 [128, 32], P('ep', 'tp'), may hold values from -3 to 3
- w_mix_out: bfloat16 [2048, 4096], P('tp'), may hold values from -0.125 to 0.125
- ffn_gain: float32 [4096], replicated, may hold values from 0.1 to 1.9
- routes: int32 [128, 2], replicated, may hold values from 0 to 7, all different within a row; in each aligned block of 32 rows (0 to 31, 32 to 63, ...) at most 9 rows name the same one
- route_weights: float32 [128, 2], P('ep'), may hold values from 0.1 to 1
- expert_gate: bfloat16 [8, 4096, 2048], P('ep', None, 'tp'), may hold values from -0.09375 to 0.09375
- expert_up: bfloat16 [8, 4096, 2048], P('ep', None, 'tp'), may hold values from -0.09375 to 0.09375
- expert_down: bfloat16 [8, 2048, 4096], P('ep', 'tp'), may hold values from -0.125 to 0.125
- shared_gate: bfloat16 [4096, 1024], P(None, 'tp'), may hold values from -0.09375 to 0.09375
- shared_up: bfloat16 [4096, 1024], P(None, 'tp'), may hold values from -0.09375 to 0.09375
- shared_down: bfloat16 [1024, 4096], P('tp'), may hold values from -0.1875 to 0.1875
Outputs:
- result: bfloat16 [128, 4096], P('ep', 'tp')
- new_matrix: float32 [128, 32, 64, 64], P('ep', 'tp')
- new_norm: float32 [128, 32, 64], P('ep', 'tp')
- new_max: float32 [128, 32], P('ep', 'tp')
Inputs may be any that keep to these rules, and one draw needn't show every extreme that they name: `routes`: each row names 2 different experts. In each aligned block of 32 rows (the rows of one device group along ep) no expert is named by more than 9 rows, a bound that some block reaches.
All inputs are finite; a program needn't handle non-finite values.
Results may differ from a plain program's by a relative error of at most 0.023.
Values may be sent and summed in bfloat16 or wider, within the bound.
A program may use at most 64 MiB of HBM per device.

v0:
```python
import jax
import jax.numpy as jnp
from jax import lax
from jax.sharding import PartitionSpec as P

norm_eps = 1e-06


def rms_scale(inputs, scales):
    floats = inputs.astype(jnp.float32)
    return floats * lax.rsqrt(jnp.mean(floats * floats, -1, keepdims=True) + norm_eps) * scales


def slot_ranks(chosen, experts):
    flat_ids = chosen.reshape(-1)
    onehot = (flat_ids[:, None] == jnp.arange(experts, dtype=jnp.int32)[None, :]).astype(jnp.int32)
    earlier = jnp.cumsum(onehot, 0) - onehot
    return jnp.sum(earlier * onehot, 1).reshape(chosen.shape)


def per_device(
    hidden_in,
    mix_gain,
    w_query,
    w_key,
    w_value,
    w_outgate,
    w_gates,
    gate_bias,
    state_matrix,
    state_norm,
    state_max,
    w_mix_out,
    ffn_gain,
    routes,
    route_weights,
    expert_gate,
    expert_up,
    expert_down,
    shared_gate,
    shared_up,
    shared_down,
):
    ep_count = lax.axis_size("ep")
    tp_count = lax.axis_size("tp")
    group_index = lax.axis_index("ep")
    column_index = lax.axis_index("tp")
    seq_rows, width = hidden_in.shape
    heads_dev = state_matrix.shape[1]
    head_dim = state_matrix.shape[2]
    top_count = routes.shape[1]
    local_experts = expert_gate.shape[0]
    expert_total = local_experts * ep_count
    capacity = max(2, seq_rows * top_count // expert_total + 1)
    slot_count = ep_count * capacity
    slice_width = width // tp_count
    normed = rms_scale(hidden_in, mix_gain).astype(jnp.bfloat16)
    gathered = lax.all_to_all(normed, "ep", split_axis=1, concat_axis=0, tiled=True)
    joined = jnp.concatenate([w_query, w_key, w_value, w_outgate], 1)
    projected = lax.psum_scatter(
        jnp.dot(gathered, joined, preferred_element_type=jnp.float32).astype(jnp.bfloat16),
        "ep",
        scatter_dimension=0,
        tiled=True,
    )
    head_cols = heads_dev * head_dim

    def heads_of(role_index):
        part = projected[:, role_index * head_cols : (role_index + 1) * head_cols]
        return part.astype(jnp.float32).reshape(seq_rows, heads_dev, head_dim)

    query_heads = heads_of(0)
    key_heads = heads_of(1) * head_dim ** (-0.5)
    value_heads = heads_of(2)
    out_gate = heads_of(3)
    gate_pre = jnp.einsum("sd,gdh->gsh", normed, w_gates, preferred_element_type=jnp.float32)
    gate_pre = gate_pre + gate_bias[:, None, :]
    carried = jax.nn.log_sigmoid(gate_pre[1]) + state_max
    new_max = jnp.maximum(carried, gate_pre[0])
    forget_weight = jnp.exp(carried - new_max)[..., None]
    input_weight = jnp.exp(gate_pre[0] - new_max)[..., None]
    new_norm = forget_weight * state_norm + input_weight * key_heads
    new_matrix = (
        forget_weight[..., None] * state_matrix
        + (input_weight * value_heads)[..., :, None] * key_heads[..., None, :]
    )
    numerator = jnp.einsum(
        "shek,shk->she", new_matrix, query_heads, precision=lax.Precision.HIGHEST
    )
    denominator = jnp.maximum(jnp.abs(jnp.sum(new_norm * query_heads, -1)), 1.0)
    gated_out = (jax.nn.sigmoid(out_gate) * numerator / denominator[..., None]).reshape(
        seq_rows, head_cols
    )
    gated_out = gated_out.astype(jnp.bfloat16)
    mixed_part = jnp.dot(gated_out, w_mix_out, preferred_element_type=jnp.float32)
    mixed_own = lax.psum_scatter(
        mixed_part.astype(jnp.bfloat16), "tp", scatter_dimension=1, tiled=True
    ).astype(jnp.float32)
    residual_own = lax.dynamic_slice_in_dim(hidden_in, column_index * slice_width, slice_width, 1)
    stream_own = (residual_own.astype(jnp.float32) + mixed_own).astype(jnp.bfloat16)
    stream = lax.all_gather(stream_own, "tp", axis=1, tiled=True)
    ffn_in = rms_scale(stream, ffn_gain).astype(jnp.bfloat16)
    shared_hidden = (
        jax.nn.silu(jnp.dot(ffn_in, shared_gate, preferred_element_type=jnp.float32))
        * jnp.dot(ffn_in, shared_up, preferred_element_type=jnp.float32)
    ).astype(jnp.bfloat16)
    shared_part = jnp.dot(shared_hidden, shared_down, preferred_element_type=jnp.float32)
    own_routes = lax.dynamic_slice_in_dim(routes, group_index * seq_rows, seq_rows, 0)
    slot_ids = own_routes * capacity + slot_ranks(own_routes, expert_total)
    slot_range = jnp.arange(expert_total * capacity, dtype=jnp.int32)
    matches = slot_ids[:, :, None] == slot_range[None, None, :]
    chooser = jnp.any(matches, 1).astype(jnp.bfloat16)
    outgoing = jnp.einsum("sj,sd->jd", chooser, ffn_in, preferred_element_type=jnp.float32)
    outgoing = outgoing.astype(jnp.bfloat16).reshape(expert_total, capacity, width)
    arrived = lax.all_to_all(outgoing, "ep", split_axis=0, concat_axis=1, tiled=True)
    gate_values = jnp.einsum(
        "erd,edf->erf", arrived, expert_gate, preferred_element_type=jnp.float32
    )
    up_values = jnp.einsum("erd,edf->erf", arrived, expert_up, preferred_element_type=jnp.float32)
    expert_hidden = (jax.nn.silu(gate_values) * up_values).astype(jnp.bfloat16)
    expert_part = jnp.einsum(
        "erf,efd->erd", expert_hidden, expert_down, preferred_element_type=jnp.float32
    )
    expert_part = expert_part.reshape(local_experts * slot_count, width)
    routed_sum, shared_sum = (
        lax.psum_scatter(
            expert_part.astype(jnp.bfloat16), "tp", scatter_dimension=1, tiled=True
        ).astype(jnp.float32),
        lax.psum_scatter(
            shared_part.astype(jnp.bfloat16), "tp", scatter_dimension=1, tiled=True
        ).astype(jnp.float32),
    )
    expert_rows = routed_sum.astype(jnp.bfloat16)
    returned = lax.all_to_all(
        expert_rows.reshape(local_experts, slot_count, slice_width),
        "ep",
        split_axis=1,
        concat_axis=0,
        tiled=True,
    )
    returned = returned.reshape(expert_total * capacity, slice_width)
    weights = jnp.sum(jnp.where(matches, route_weights[:, :, None], 0.0), 1)
    routed = jnp.dot(weights, returned.astype(jnp.float32), precision=lax.Precision.HIGHEST)
    result = (stream_own.astype(jnp.float32) + shared_sum + routed).astype(jnp.bfloat16)
    return (result, new_matrix, new_norm, new_max)


def solution(mesh):
    placed = (
        P("ep", None),
        P(),
        P("ep", "tp"),
        P("ep", "tp"),
        P("ep", "tp"),
        P("ep", "tp"),
        P(None, None, "tp"),
        P(None, "tp"),
        P("ep", "tp", None, None),
        P("ep", "tp", None),
        P("ep", "tp"),
        P("tp", None),
        P(),
        P(),
        P("ep", None),
        P("ep", None, "tp"),
        P("ep", None, "tp"),
        P("ep", "tp", None),
        P(None, "tp"),
        P(None, "tp"),
        P("tp", None),
    )
    return jax.shard_map(
        per_device,
        mesh=mesh,
        in_specs=placed,
        out_specs=(P("ep", "tp"), P("ep", "tp", None, None), P("ep", "tp", None), P("ep", "tp")),
        check_vma=False,
    )
```

profile of v0, /device:TPU:0, one launch (start us, length us, event | category | flops | bytes accessed | tf_op | source)
XLA Modules:
  0.0 207.5 jit_solution(7990342096338553955)
XLA Ops:
  7.2 1.3 fusion.19
  8.4 1.1 fusion.21
  9.5 0.7 copy.88
  10.3 5.2 %all-to-all-start = ((bf16[32,4,1024]{2,0,1:T(8,128)(2,1)}), bf16[32,4,1024]{2,0,1:T(8,128)(2,1)S(1)}, u32[]{:S(2)}, u32[]{:S(2)}) async-start(bf16[32,4,1024]{2,0,1:T(8,128)(2,1)} %bitcast.53), calls=%async_computation | async-start | bytes 524288 | tf_op jit(solution)/shard_map/all_to_all | solution.py:58
  15.5 1.0 fusion.14
  16.5 4.3 %all-to-all-done = bf16[32,4,1024]{2,0,1:T(8,128)(2,1)S(1)} async-done(((bf16[32,4,1024]{2,0,1:T(8,128)(2,1)}), bf16[32,4,1024]{2,0,1:T(8,128)(2,1)S(1)}, u32[]{:S(2)}, u32[]{:S(2)}) %all-to-all-start) | async-done | bytes 262176 | tf_op jit(solution)/shard_map/all_to_all | solution.py:58
  20.8 2.7 %fusion.8 = bf16[128,1024]{1,0:T(8,128)(2,1)} fusion(bf16[128,1024]{1,0:T(8,128)(2,1)S(1)} %bitcast.60, bf16[1024,256]{1,0:T(8,128)(2,1)} %param.26, bf16[1024,256]{1,0:T(8,128)(2,1)} %param.25, bf16[1024,256]{1,0:T(8,128)(2,1)} %param.24, bf16[1024,256]{1,0:T(8,128)(2,1)} %param.23), kind=kOutput, calls=%fused_computation.13 | convolution fusion | flops 276955136 | bytes 2621440 | tf_op jit(solution)/shard_map/dot_general | solution.py:61
  23.7 0.1 copy.67
  24.0 0.1 copy.80
  24.1 0.1 eq.28
  24.2 23.9 %reduce-scatter.5.cloned.1.call-done = bf16[32,1024]{1,0:T(8,128)(2,1)} async-done(((bf16[128,1024]{1,0:T(8,128)(2,1)}), bf16[32,1024]{1,0:T(8,128)(2,1)}) %reduce-scatter.5.cloned.1.call-update) | async-done | bytes 65552 | tf_op jit(solution)/shard_map/reduce_scatter | solution.py:60
  48.1 0.8 fusion.54
  48.9 0.1 reshape.97
  49.0 0.1 reshape.111
  49.1 0.1 reshape.104
  49.2 0.1 reshape.106
  49.3 0.8 multiply_reduce_fusion
  50.1 0.7 add_divide_fusion
  50.8 0.1 div.30
  50.9 3.7 %multiply_add_fusion = f32[32,4,64,64]{3,2,1,0:T(8,128)S(1)} fusion(f32[32,4,64,64]{3,2,1,0:T(8,128)} %param.29, f32[32,4,64]{2,1,0:T(4,128)S(1)} %get-tuple-element.9, f32[32,4,64]{2,1,0:T(4,128)S(1)} %get-tuple-element.13, f32[32,4]{1,0:T(8,128)S(1)} %copy.67), kind=kLoop, calls=%fused_computation.4 | loop fusion | flops 1572864 | bytes 4260352 | tf_op jit(solution)/shard_map/add | solution.py:84
  54.7 2.0 copy-done.1
  56.7 3.4 %fusion.55 = f32[32,4,1,64]{3,2,1,0:T(1,128)S(1)} fusion(f32[32,4,64,64]{3,2,1,0:T(8,128)S(1)} %multiply_add_fusion, bf16[32,4,64,1]{2,3,1,0:T(2,128)(2,1)S(1)} %reshape.111), kind=kOutput, calls=%fused_computation.85 | convolution fusion | flops 6291456 | bytes 2146304 | tf_op jit(solution)/shard_map/shek,shk->she/dot_general | solution.py:87
  60.0 0.1 fusion.31
  60.1 0.1 convert_element_type.79
  60.3 1.2 convolution_convert_fusion.3
  61.6 0.1 reduce_window_sum.11
  61.7 0.2 select_reduce_fusion.1
  61.8 0.1 reshape.99
  62.1 30.2 %reduce-scatter.7.cloned.1.call-done = bf16[32,512]{1,0:T(8,128)(2,1)} async-done(((bf16[32,4096]{1,0:T(8,128)(2,1)}), bf16[32,512]{1,0:T(8,128)(2,1)}) %reduce-scatter.7.cloned.1.call-update) | async-done | bytes 32784 | tf_op jit(solution)/shard_map/reduce_scatter | solution.py:96
  92.3 0.8 add_convert_fusion
  93.1 14.2 %all_gather.3 = bf16[32,4096]{1,0:T(8,128)(2,1)S(1)} all-gather(bf16[32,512]{1,0:T(8,128)(2,1)S(1)} %add_convert_fusion), channel_id=1, replica_groups=mesh['ep'=4,'tp'=8] {'tp'}, dimensions={1}, use_global_device_ids=true | all-gather | bytes 294912 | tf_op jit(solution)/shard_map/all_gather | solution.py:101
  107.3 0.2 fusion.22
  107.5 1.2 convolution_convert_fusion.1
  108.7 1.3 reshape.100
  110.0 18.2 %all_to_all.52 = bf16[8,9,4096]{2,1,0:T(8,128)(2,1)S(1)} all-to-all(bf16[8,9,4096]{2,1,0:T(8,128)(2,1)S(1)} %reshape.100), channel_id=1, replica_groups=mesh['ep'=4,'tp'=8] {'ep'}, dimensions={0} | all-to-all | bytes 1179648 | tf_op jit(solution)/shard_map/all_to_all | solution.py:115
  128.2 0.6 copy.73
  128.8 3.1 %fusion.17 = f32[2,36,256]{2,1,0:T(8,128)S(1)} fusion(bf16[2,4096,256]{2,1,0:T(8,128)(2,1)} %param.36, bf16[2,36,4096]{2,0,1:T(2,128)(2,1)S(1)} %bitcast.54), kind=kOutput, calls=%fused_computation.27 | convolution fusion | flops 150994944 | bytes 4857856 | tf_op jit(solution)/shard_map/erd,edf->erf/dot_general | solution.py:116
  131.9 6.0 %convolution_convert_fusion = bf16[2,36,4096]{2,1,0:T(8,128)(2,1)} fusion(bf16[2,256,4096]{2,1,0:T(8,128)(2,1)} %param.38, bf16[2,4096,256]{2,1,0:T(8,128)(2,1)} %param.37, bf16[2,36,4096]{2,0,1:T(2,128)(2,1)S(1)} %bitcast.55, f32[2,36,256]{2,1,0:T(8,128)S(1)} %fusion.17), kind=kOutput, calls=%fused_computation | convolution fusion | flops 302395392 | bytes 9641984 | tf_op jit(solution)/shard_map/erf,efd->erd/dot_general | solution.py:121
  137.9 2.0 convert_element_type.93
  140.0 1.6 fusion.51
  141.6 2.9 %convolution_convert_fusion.2 = bf16[32,4096]{1,0:T(8,128)(2,1)} fusion(bf16[128,4096]{1,0:T(8,128)(2,1)} %param.41, bf16[4096,128]{1,0:T(8,128)(2,1)} %param.40, f32[32,128]{1,0:T(8,128)S(1)} %fusion.51, bf16[32,4096]{1,0:T(8,128)(2,1)S(1)} %all_gather.3, f32[4096]{0:T(1024)S(1)} %copy-done.2, f32[32]{0:T(128)S(1)} %add_rsqrt_fusion), kind=kOutput, calls=%fused_computation.2 | convolution fusion | flops 67788800 | bytes 2654336 | tf_op jit(solution)/shard_map/dot_general | solution.py:107
  144.5 23.9 %reduce-scatter.11.cloned.1.call-done = bf16[72,512]{1,0:T(8,128)(2,1)} async-done(((bf16[72,4096]{1,0:T(8,128)(2,1)}), bf16[72,512]{1,0:T(8,128)(2,1)}) %reduce-scatter.11.cloned.1.call-update) | async-done | bytes 73744 | tf_op jit(solution)/shard_map/reduce_scatter | solution.py:126
  168.4 0.9 reshape.101
  169.3 0.7 copy.76
  170.0 3.6 %all-to-all-start.2 = ((bf16[2,36,512]{2,0,1:T(2,128)(2,1)}), bf16[2,36,512]{2,0,1:T(2,128)(2,1)S(1)}, u32[]{:S(2)}, u32[]{:S(2)}) async-start(bf16[2,36,512]{2,0,1:T(2,128)(2,1)} %copy.76), calls=%async_computation.6 | async-start | bytes 147456 | tf_op jit(solution)/shard_map/all_to_all | solution.py:134
  173.7 4.8 %all-to-all-done.2 = bf16[2,36,512]{2,0,1:T(2,128)(2,1)S(1)} async-done(((bf16[2,36,512]{2,0,1:T(2,128)(2,1)}), bf16[2,36,512]{2,0,1:T(2,128)(2,1)S(1)}, u32[]{:S(2)}, u32[]{:S(2)}) %all-to-all-start.2) | async-done | bytes 73760 | tf_op jit(solution)/shard_map/all_to_all | solution.py:134
  178.5 20.9 %reduce-scatter.9.cloned.1.call-done = bf16[32,512]{1,0:T(8,128)(2,1)} async-done(((bf16[32,4096]{1,0:T(8,128)(2,1)}), bf16[32,512]{1,0:T(8,128)(2,1)}) %reduce-scatter.9.cloned.1.call-update) | async-done | bytes 32784 | tf_op jit(solution)/shard_map/reduce_scatter | solution.py:129
  199.4 1.5 fusion.12
  (38 shorter events, 0.9 us)
Async XLA Ops:
  7.2 53.1 %copy-start = (bf16[256,4096]{1,0:T(8,128)(2,1)S(1)}, bf16[256,4096]{1,0:T(8,128)(2,1)}, u32[]{:S(2)}) copy-start(bf16[256,4096]{1,0:T(8,128)(2,1)} %param.32) | copy-start | bytes 6291460
  10.3 10.6 %all-to-all-start = ((bf16[32,4,1024]{2,0,1:T(8,128)(2,1)}), bf16[32,4,1024]{2,0,1:T(8,128)(2,1)S(1)}, u32[]{:S(2)}, u32[]{:S(2)}) async-start(bf16[32,4,1024]{2,0,1:T(8,128)(2,1)} %bitcast.53), calls=%async_computation | async-start | bytes 524288 | tf_op jit(solution)/shard_map/all_to_all | solution.py:58
  15.5 32.7 %reduce-scatter.5.cloned.1.call-start = ((), (), s32[]{:S(2)}) async-start(), calls=%async_computation.7 | async-start | bytes 327680 | tf_op jit(solution)/shard_map/reduce_scatter | solution.py:60
  16.5 7.1 %copy-start.4 = (f32[32,4]{0,1:T(4,128)S(1)}, f32[32,4]{0,1:T(4,128)}, u32[]{:S(2)}) copy-start(f32[32,4]{0,1:T(4,128)} %param.31) | copy-start | bytes 1540
  20.8 3.1 %copy-start.7 = (s32[128,2]{0,1:T(2,128)S(1)}, s32[128,2]{0,1:T(2,128)}, u32[]{:S(2)}) copy-start(s32[128,2]{0,1:T(2,128)} %param.34) | copy-start | bytes 3076
  20.8 28.4 %copy-start.3 = (f32[32,4,64]{2,1,0:T(4,128)S(1)}, f32[32,4,64]{2,1,0:T(4,128)}, u32[]{:S(2)}) copy-start(f32[32,4,64]{2,1,0:T(4,128)} %param.30) | copy-start | bytes 98308
  23.6 68.8 %reduce-scatter.7.cloned.1.call-start = ((), (), s32[]{:S(2)}) async-start(), calls=%async_computation.8 | async-start | bytes 294912 | tf_op jit(solution)/shard_map/reduce_scatter | solution.py:96
  23.6 31.0 %copy-start.5 = (f32[32,4]{0,1:T(4,128)}, f32[32,4]{0,1:T(4,128)S(1)}, u32[]{:S(2)}) copy-start(f32[32,4]{0,1:T(4,128)S(1)} %get-tuple-element.8) | copy-start | bytes 1540
  54.6 2.0 copy-start.1
  56.7 50.8 %copy-start.2 = (f32[4096]{0:T(1024)S(1)}, f32[4096]{0:T(1024)}, u32[]{:S(2)}) copy-start(f32[4096]{0:T(1024)} %param.33) | copy-start | bytes 49156
  61.4 106.9 %reduce-scatter.11.cloned.1.call-start = ((), (), s32[]{:S(2)}) async-start(), calls=%async_computation.10 | async-start | bytes 663552 | tf_op jit(solution)/shard_map/reduce_scatter | solution.py:126
  137.9 35.7 %copy-start.6 = (f32[32,2]{0,1:T(2,128)S(1)}, f32[32,2]{0,1:T(2,128)}, u32[]{:S(2)}) copy-start(f32[32,2]{0,1:T(2,128)} %param.35) | copy-start | bytes 772
  140.0 59.4 %reduce-scatter.9.cloned.1.call-start = ((), (), s32[]{:S(2)}) async-start(), calls=%async_computation.9 | async-start | bytes 294912 | tf_op jit(solution)/shard_map/reduce_scatter | solution.py:129
  170.0 8.5 %all-to-all-start.2 = ((bf16[2,36,512]{2,0,1:T(2,128)(2,1)}), bf16[2,36,512]{2,0,1:T(2,128)(2,1)S(1)}, u32[]{:S(2)}, u32[]{:S(2)}) async-start(bf16[2,36,512]{2,0,1:T(2,128)(2,1)} %copy.76), calls=%async_computation.6 | async-start | bytes 147456 | tf_op jit(solution)/shard_map/all_to_all | solution.py:134
Sparse Core Ops, SparseCore 0:
  23.7 24.3 reduce-scatter.4
  61.6 30.7 reduce-scatter.6
  140.1 28.2 reduce-scatter.10
  170.5 28.9 reduce-scatter.8
where the time goes:
time: 208 us
  waiting for transfers between devices  108 us (52%)
  blocking collectives  32.4 us (16%)
  matrix products  24.5 us (12%)
  between operations  14 us (7%)
  other arithmetic  10 us (5%)
  local copies, waits for them, and re-layouts  9.69 us (5%)
  starting transfers between devices  8.96 us (4%)
    reduce_scatter x1, waiting for transfers between devices, per_device(): lax.psum_scatter(mixed_part.astype(jnp.bfloat16), 'tp', scatter_dimension...  30.2 us
    reduce_scatter x1, waiting for transfers between devices, per_device(): lax.psum_scatter(jnp.dot(gathered, joined, preferred_element_type=jnp.flo...  23.9 us
    reduce_scatter x1, waiting for transfers between devices, per_device(): lax.psum_scatter(expert_part.astype(jnp.bfloat16), 'tp', scatter_dimensio...  23.9 us
    reduce_scatter x1, waiting for transfers between devices, per_device(): lax.psum_scatter(shared_part.astype(jnp.bfloat16), 'tp', scatter_dimensio...  20.9 us
    all_to_all x1, blocking collectives, per_device(): lax.all_to_all(outgoing, 'ep', split_axis=0, concat_axis=1, tiled=True)  18.2 us
    all_gather x1, blocking collectives, per_device(): stream = lax.all_gather(stream_own, 'tp', axis=1, tiled=True)  14.2 us
    dot_general x1, matrix products, per_device(): jnp.einsum('erf,efd->erd', expert_hidden, expert_down, preferred_element_...  6.02 us
    all_to_all x1, starting transfers between devices, per_device(): lax.all_to_all(normed, 'ep', split_axis=1, concat_axis=0, tiled=True)  5.19 us
  transfers between devices with their start and end apart: 6, of which 6 were waited for; matrix products, arithmetic and copies ran while one was open for 4% of the time, Pallas kernels for 0%

commit v1 on v0

--- a/solution.py
+++ b/solution.py
@@ -112,7 +112,10 @@
     chooser = jnp.any(matches, 1).astype(jnp.bfloat16)
     outgoing = jnp.einsum("sj,sd->jd", chooser, ffn_in, preferred_element_type=jnp.float32)
     outgoing = outgoing.astype(jnp.bfloat16).reshape(expert_total, capacity, width)
-    arrived = lax.all_to_all(outgoing, "ep", split_axis=0, concat_axis=1, tiled=True)
+    arrived = jnp.concatenate(
+        lax.all_to_all(jnp.stack(jnp.split(outgoing, lax.axis_size("ep"), axis=0)), "ep", 0, 0),
+        axis=1,
+    )
     gate_values = jnp.einsum(
         "erd,edf->erf", arrived, expert_gate, preferred_element_type=jnp.float32
     )

time: 208 us -> 201 us (0.966)
  blocking collectives: 32.4 us -> 27.8 us
  matrix products: 24.5 us -> 21.5 us
    all_to_all x1, blocking collectives: 18.2 us -> 13.6 us  [per_device(): lax.all_to_all(jnp.stack(jnp.split(outgoing, lax.axis_size('ep'), axis=0)...]
    dot_general x1, matrix products: 3.1 us -> 0.92 us  [per_device(): jnp.einsum('erd,edf->erf', arrived, expert_gate, preferred_element_type=j...]
where the time goes in v1:
time: 201 us
  waiting for transfers between devices  108 us (54%)
  blocking collectives  27.8 us (14%)
  matrix products  21.5 us (11%)
  between operations  14 us (7%)
  local copies, waits for them, and re-layouts  10.3 us (5%)
  other arithmetic  10.2 us (5%)
  starting transfers between devices  8.81 us (4%)
    reduce_scatter x1, waiting for transfers between devices, per_device(): lax.psum_scatter(mixed_part.astype(jnp.bfloat16), 'tp', scatter_dimension...  30.2 us
    reduce_scatter x1, waiting for transfers between devices, per_device(): lax.psum_scatter(jnp.dot(gathered, joined, preferred_element_type=jnp.flo...  23.9 us
    reduce_scatter x1, waiting for transfers between devices, per_device(): lax.psum_scatter(expert_part.astype(jnp.bfloat16), 'tp', scatter_dimensio...  23.7 us
    reduce_scatter x1, waiting for transfers between devices, per_device(): lax.psum_scatter(shared_part.astype(jnp.bfloat16), 'tp', scatter_dimensio...  20.9 us
    all_gather x1, blocking collectives, per_device(): stream = lax.all_gather(stream_own, 'tp', axis=1, tiled=True)  14.2 us
    all_to_all x1, blocking collectives, per_device(): lax.all_to_all(jnp.stack(jnp.split(outgoing, lax.axis_size('ep'), axis=0)...  13.6 us
    dot_general x1, matrix products, per_device(): jnp.einsum('erf,efd->erd', expert_hidden, expert_down, preferred_element_...  6.02 us
    all_to_all x1, starting transfers between devices, per_device(): lax.all_to_all(normed, 'ep', split_axis=1, concat_axis=0, tiled=True)  5.19 us
  transfers between devices with their start and end apart: 6, of which 6 were waited for; matrix products, arithmetic and copies ran while one was open for 4% of the time, Pallas kernels for 0%

profile of v1, /device:TPU:0, one launch (start us, length us, event | category | flops | bytes accessed | tf_op | source)
XLA Modules:
  0.0 200.5 jit_solution(15536689283948842198)
XLA Ops:
  7.2 1.3 fusion.19
  8.4 1.1 fusion.21
  9.5 0.7 copy.88
  10.3 5.2 %all-to-all-start = ((bf16[32,4,1024]{2,0,1:T(8,128)(2,1)}), bf16[32,4,1024]{2,0,1:T(8,128)(2,1)S(1)}, u32[]{:S(2)}, u32[]{:S(2)}) async-start(bf16[32,4,1024]{2,0,1:T(8,128)(2,1)} %bitcast.52), calls=%async_computation | async-start | bytes 524288 | tf_op jit(solution)/shard_map/all_to_all | solution.py:58
  15.5 1.0 fusion.14
  16.5 4.3 %all-to-all-done = bf16[32,4,1024]{2,0,1:T(8,128)(2,1)S(1)} async-done(((bf16[32,4,1024]{2,0,1:T(8,128)(2,1)}), bf16[32,4,1024]{2,0,1:T(8,128)(2,1)S(1)}, u32[]{:S(2)}, u32[]{:S(2)}) %all-to-all-start) | async-done | bytes 262176 | tf_op jit(solution)/shard_map/all_to_all | solution.py:58
  20.8 2.7 %fusion.8 = bf16[128,1024]{1,0:T(8,128)(2,1)} fusion(bf16[128,1024]{1,0:T(8,128)(2,1)S(1)} %bitcast.58, bf16[1024,256]{1,0:T(8,128)(2,1)} %param.26, bf16[1024,256]{1,0:T(8,128)(2,1)} %param.25, bf16[1024,256]{1,0:T(8,128)(2,1)} %param.24, bf16[1024,256]{1,0:T(8,128)(2,1)} %param.23), kind=kOutput, calls=%fused_computation.13 | convolution fusion | flops 276955136 | bytes 2621440 | tf_op jit(solution)/shard_map/dot_general | solution.py:61
  24.1 0.1 eq.28
  24.2 23.9 %reduce-scatter.5.cloned.1.call-done = bf16[32,1024]{1,0:T(8,128)(2,1)} async-done(((bf16[128,1024]{1,0:T(8,128)(2,1)}), bf16[32,1024]{1,0:T(8,128)(2,1)}) %reduce-scatter.5.cloned.1.call-update) | async-done | bytes 65552 | tf_op jit(solution)/shard_map/reduce_scatter | solution.py:60
  48.1 0.8 fusion.55
  48.9 0.1 reshape.109
  49.0 0.1 reshape.124
  49.1 0.1 reshape.117
  49.2 0.1 reshape.119
  49.3 0.8 multiply_reduce_fusion
  50.1 0.7 add_divide_fusion
  50.8 0.1 div.30
  50.9 3.7 %multiply_add_fusion = f32[32,4,64,64]{3,2,1,0:T(8,128)S(1)} fusion(f32[32,4,64,64]{3,2,1,0:T(8,128)} %param.29, f32[32,4,64]{2,1,0:T(4,128)S(1)} %get-tuple-element.13, f32[32,4,64]{2,1,0:T(4,128)S(1)} %get-tuple-element.17, f32[32,4]{1,0:T(8,128)S(1)} %copy.67), kind=kLoop, calls=%fused_computation.4 | loop fusion | flops 1572864 | bytes 4260352 | tf_op jit(solution)/shard_map/add | solution.py:84
  54.7 2.0 copy-done.1
  56.7 3.4 %fusion.56 = f32[32,4,1,64]{3,2,1,0:T(1,128)S(1)} fusion(f32[32,4,64,64]{3,2,1,0:T(8,128)S(1)} %multiply_add_fusion, bf16[32,4,64,1]{2,3,1,0:T(2,128)(2,1)S(1)} %reshape.124), kind=kOutput, calls=%fused_computation.87 | convolution fusion | flops 6291456 | bytes 2146304 | tf_op jit(solution)/shard_map/shek,shk->she/dot_general | solution.py:87
  60.0 0.1 fusion.31
  60.1 0.1 convert_element_type.79
  60.3 1.2 convolution_convert_fusion.3
  61.6 0.1 reduce_window_sum.11
  61.7 0.2 select_reduce_fusion.1
  61.8 0.1 reshape.111
  62.1 30.2 %reduce-scatter.7.cloned.1.call-done = bf16[32,512]{1,0:T(8,128)(2,1)} async-done(((bf16[32,4096]{1,0:T(8,128)(2,1)}), bf16[32,512]{1,0:T(8,128)(2,1)}) %reduce-scatter.7.cloned.1.call-update) | async-done | bytes 32784 | tf_op jit(solution)/shard_map/reduce_scatter | solution.py:96
  92.3 0.8 add_convert_fusion
  93.1 14.2 %all_gather.3 = bf16[32,4096]{1,0:T(8,128)(2,1)S(1)} all-gather(bf16[32,512]{1,0:T(8,128)(2,1)S(1)} %add_convert_fusion), channel_id=1, replica_groups=mesh['ep'=4,'tp'=8] {'tp'}, dimensions={1}, use_global_device_ids=true | all-gather | bytes 294912 | tf_op jit(solution)/shard_map/all_gather | solution.py:101
  107.3 0.2 fusion.22
  107.5 0.4 convolution_convert_fusion.1
  107.9 0.8 fusion.54
  108.8 1.0 stack.18
  109.8 0.2 pad_maximum_fusion
  110.0 0.6 copy.73
  110.7 13.6 %all_to_all.39 = bf16[4,2,9,4096]{3,1,2,0:T(2,128)(2,1)S(1)} all-to-all(bf16[4,2,9,4096]{3,1,2,0:T(2,128)(2,1)S(1)} %copy.73), channel_id=1, replica_groups=mesh['ep'=4,'tp'=8] {'ep'}, dimensions={0} | all-to-all | bytes 1179648 | tf_op jit(solution)/shard_map/all_to_all | solution.py:116
  124.3 0.9 fusion.17
  125.2 6.0 %convolution_convert_fusion = bf16[2,36,4096]{2,1,0:T(8,128)(2,1)} fusion(bf16[2,256,4096]{2,1,0:T(8,128)(2,1)} %param.38, bf16[2,4096,256]{2,1,0:T(8,128)(2,1)} %param.37, bf16[2,36,4096]{2,0,1:T(2,128)(2,1)S(1)} %bitcast.54, f32[2,36,256]{2,1,0:T(8,128)S(1)} %fusion.17), kind=kOutput, calls=%fused_computation | convolution fusion | flops 302395392 | bytes 9641984 | tf_op jit(solution)/shard_map/erf,efd->erd/dot_general | solution.py:124
  131.2 2.0 %convert_element_type.93 = bf16[72,4096]{1,0:T(8,128)(2,1)} reshape(bf16[2,36,4096]{2,1,0:T(8,128)(2,1)} %convolution_convert_fusion) | data formatting | bytes 1179648 | tf_op jit(solution)/shard_map/convert_element_type | solution.py:130
  133.3 1.6 fusion.51
  134.9 2.9 %convolution_convert_fusion.2 = bf16[32,4096]{1,0:T(8,128)(2,1)} fusion(bf16[128,4096]{1,0:T(8,128)(2,1)} %param.41, bf16[4096,128]{1,0:T(8,128)(2,1)} %param.40, f32[32,128]{1,0:T(8,128)S(1)} %fusion.51, bf16[32,4096]{1,0:T(8,128)(2,1)S(1)} %all_gather.3, f32[4096]{0:T(1024)S(1)} %copy-done.3, f32[32]{0:T(128)S(1)} %add_rsqrt_fusion), kind=kOutput, calls=%fused_computation.2 | convolution fusion | flops 67788800 | bytes 2654336 | tf_op jit(solution)/shard_map/dot_general | solution.py:107
  137.8 23.7 %reduce-scatter.11.cloned.1.call-done = bf16[72,512]{1,0:T(8,128)(2,1)} async-done(((bf16[72,4096]{1,0:T(8,128)(2,1)}), bf16[72,512]{1,0:T(8,128)(2,1)}) %reduce-scatter.11.cloned.1.call-update) | async-done | bytes 73744 | tf_op jit(solution)/shard_map/reduce_scatter | solution.py:129
  161.5 0.9 reshape.114
  162.4 0.7 copy.76
  163.1 3.5 %all-to-all-start.2 = ((bf16[2,36,512]{2,0,1:T(2,128)(2,1)}), bf16[2,36,512]{2,0,1:T(2,128)(2,1)S(1)}, u32[]{:S(2)}, u32[]{:S(2)}) async-start(bf16[2,36,512]{2,0,1:T(2,128)(2,1)} %copy.76), calls=%async_computation.6 | async-start | bytes 147456 | tf_op jit(solution)/shard_map/all_to_all | solution.py:137
  166.7 4.8 %all-to-all-done.2 = bf16[2,36,512]{2,0,1:T(2,128)(2,1)S(1)} async-done(((bf16[2,36,512]{2,0,1:T(2,128)(2,1)}), bf16[2,36,512]{2,0,1:T(2,128)(2,1)S(1)}, u32[]{:S(2)}, u32[]{:S(2)}) %all-to-all-start.2) | async-done | bytes 73760 | tf_op jit(solution)/shard_map/all_to_all | solution.py:137
  171.5 20.9 %reduce-scatter.9.cloned.1.call-done = bf16[32,512]{1,0:T(8,128)(2,1)} async-done(((bf16[32,4096]{1,0:T(8,128)(2,1)}), bf16[32,512]{1,0:T(8,128)(2,1)}) %reduce-scatter.9.cloned.1.call-update) | async-done | bytes 32784 | tf_op jit(solution)/shard_map/reduce_scatter | solution.py:132
  192.4 1.5 fusion.12
  (45 shorter events, 1.3 us)
Async XLA Ops:
  7.2 53.1 %copy-start = (bf16[256,4096]{1,0:T(8,128)(2,1)S(1)}, bf16[256,4096]{1,0:T(8,128)(2,1)}, u32[]{:S(2)}) copy-start(bf16[256,4096]{1,0:T(8,128)(2,1)} %param.32) | copy-start | bytes 6291460
  10.3 10.6 %all-to-all-start = ((bf16[32,4,1024]{2,0,1:T(8,128)(2,1)}), bf16[32,4,1024]{2,0,1:T(8,128)(2,1)S(1)}, u32[]{:S(2)}, u32[]{:S(2)}) async-start(bf16[32,4,1024]{2,0,1:T(8,128)(2,1)} %bitcast.52), calls=%async_computation | async-start | bytes 524288 | tf_op jit(solution)/shard_map/all_to_all | solution.py:58
  15.5 32.7 %reduce-scatter.5.cloned.1.call-start = ((), (), s32[]{:S(2)}) async-start(), calls=%async_computation.7 | async-start | bytes 327680 | tf_op jit(solution)/shard_map/reduce_scatter | solution.py:60
  16.5 7.1 %copy-start.5 = (f32[32,4]{0,1:T(4,128)S(1)}, f32[32,4]{0,1:T(4,128)}, u32[]{:S(2)}) copy-start(f32[32,4]{0,1:T(4,128)} %param.31) | copy-start | bytes 1540
  20.8 3.1 %copy-start.8 = (s32[128,2]{0,1:T(2,128)S(1)}, s32[128,2]{0,1:T(2,128)}, u32[]{:S(2)}) copy-start(s32[128,2]{0,1:T(2,128)} %param.34) | copy-start | bytes 3076
  20.8 28.4 %copy-start.4 = (f32[32,4,64]{2,1,0:T(4,128)S(1)}, f32[32,4,64]{2,1,0:T(4,128)}, u32[]{:S(2)}) copy-start(f32[32,4,64]{2,1,0:T(4,128)} %param.30) | copy-start | bytes 98308
  23.6 68.8 %reduce-scatter.7.cloned.1.call-start = ((), (), s32[]{:S(2)}) async-start(), calls=%async_computation.8 | async-start | bytes 294912 | tf_op jit(solution)/shard_map/reduce_scatter | solution.py:96
  23.6 31.0 %copy-start.6 = (f32[32,4]{0,1:T(4,128)}, f32[32,4]{0,1:T(4,128)S(1)}, u32[]{:S(2)}) copy-start(f32[32,4]{0,1:T(4,128)S(1)} %get-tuple-element.8) | copy-start | bytes 1540
  54.6 2.0 %copy-start.1 = (f32[32,4,64,64]{3,2,1,0:T(8,128)}, f32[32,4,64,64]{3,2,1,0:T(8,128)S(1)}, u32[]{:S(2)}) copy-start(f32[32,4,64,64]{3,2,1,0:T(8,128)S(1)} %multiply_add_fusion) | copy-start | bytes 6291460
  56.7 50.8 %copy-start.3 = (f32[4096]{0:T(1024)S(1)}, f32[4096]{0:T(1024)}, u32[]{:S(2)}) copy-start(f32[4096]{0:T(1024)} %param.33) | copy-start | bytes 49156
  61.4 100.0 %reduce-scatter.11.cloned.1.call-start = ((), (), s32[]{:S(2)}) async-start(), calls=%async_computation.10 | async-start | bytes 663552 | tf_op jit(solution)/shard_map/reduce_scatter | solution.py:129
  109.8 14.4 %copy-start.2 = (bf16[2,4096,256]{2,1,0:T(8,128)(2,1)S(1)}, bf16[2,4096,256]{2,1,0:T(8,128)(2,1)}, u32[]{:S(2)}) copy-start(bf16[2,4096,256]{2,1,0:T(8,128)(2,1)} %param.36) | copy-start | bytes 12582916
  131.2 35.4 %copy-start.7 = (f32[32,2]{0,1:T(2,128)S(1)}, f32[32,2]{0,1:T(2,128)}, u32[]{:S(2)}) copy-start(f32[32,2]{0,1:T(2,128)} %param.35) | copy-start | bytes 772
  133.3 59.2 %reduce-scatter.9.cloned.1.call-start = ((), (), s32[]{:S(2)}) async-start(), calls=%async_computation.9 | async-start | bytes 294912 | tf_op jit(solution)/shard_map/reduce_scatter | solution.py:132
  163.1 8.4 %all-to-all-start.2 = ((bf16[2,36,512]{2,0,1:T(2,128)(2,1)}), bf16[2,36,512]{2,0,1:T(2,128)(2,1)S(1)}, u32[]{:S(2)}, u32[]{:S(2)}) async-start(bf16[2,36,512]{2,0,1:T(2,128)(2,1)} %copy.76), calls=%async_computation.6 | async-start | bytes 147456 | tf_op jit(solution)/shard_map/all_to_all | solution.py:137
Sparse Core Ops, SparseCore 0:
  23.7 24.3 reduce-scatter.4
  61.6 30.7 reduce-scatter.6
  133.4 28.0 reduce-scatter.10
  163.6 28.8 reduce-scatter.8
